TPU v7x, 32 devices: a whole 2x2x4 slice. The times are simulated.
32 devices in a mesh: grp: 2 (over y), sp: 4 (over z), tp: 4 (over x, core).
Axes of the slice: x: 2, y: 2, z: 4, core: 2. Of those that a mesh axis runs over, the one named last changes fastest.
Arguments:
- query_first: bfloat16 [1536, 512], P(('grp', 'sp'), 'tp'), parts along dimension 0, may hold values from -172 to 172
- key_first: bfloat16 [1536, 512], P(('grp', 'sp'), 'tp'), parts along dimension 0, may hold values from -7.8 to 7.8
- query_second: bfloat16 [1536, 1024], P(('grp', 'sp'), 'tp'), parts along dimension 0, may hold values from -172 to 172
- key_second: bfloat16 [1536, 1024], P(('grp', 'sp'), 'tp'), parts along dimension 0, may hold values from -7.8 to 7.8
- values: bfloat16 [1536, 2, 512], P(('grp', 'sp'), None, 'tp'), parts along dimension 0, may hold values from -6 to 6
- lambdas: float32 [2, 4], P(None, 'tp'), may hold values from 0.3 to 0.8
- residual: bfloat16 [1536, 2048], P(('grp', 'sp'), 'tp'), parts along dimension 0, may hold values from -130 to 130
- norm_gain: bfloat16 [2048], P('tp'), may hold values from 0.099609375 to 1.8984375
- out_weight: bfloat16 [2, 512, 2048], P(None, 'tp'), may hold values from -0.1875 to 0.1875
- gate_weight: bfloat16 [2048, 5632], P('sp', 'tp'), may hold values from -0.125 to 0.125
- up_weight: bfloat16 [2048, 5632], P('sp', 'tp'), may hold values from -0.125 to 0.125
- down_weight: bfloat16 [5632, 2048], P('tp', 'sp'), may hold values from -0.078125 to 0.078125
Outputs:
- layer_out: bfloat16 [1536, 2048], P(('grp', 'sp'), 'tp'), parts along dimension 0
There are 2 independent parts, one for each index of `grp`. A program takes and returns all parts, laid end to end along the dimension named above; an argument that names none is the same for every part. Nothing has to cross between parts.
All inputs are finite; a program needn't handle non-finite values.
Results may differ from a plain program's by a relative error of at most 0.0065.
Values may be sent and summed in bfloat16 or wider, within the bound.
No kernel may reach another device: no remote copies, remote signals or barrier semaphores. Data moves between devices by JAX's collectives and lax.ppermute only.
A program may use at most 128 MiB of HBM per device.

v0:
```python
import jax
import jax.numpy as jnp
from jax import lax
from jax.sharding import PartitionSpec as P

D = 2048


def per_device(
    query_first,
    key_first,
    query_second,
    key_second,
    values,
    lambdas,
    residual,
    norm_gain,
    out_weight,
    gate_weight,
    up_weight,
    down_weight,
):
    tok_rows = query_first.shape[0]
    heads_here = lambdas.shape[1]
    width_first = query_first.shape[1] // (2 * heads_here)
    width_second = query_second.shape[1] // (2 * heads_here)
    value_size = values.shape[2] // heads_here
    offset = lax.axis_index("sp") * tok_rows
    query_pos = offset + lax.broadcasted_iota(jnp.int32, (tok_rows, 1), 0)
    query_groups = (
        query_first.reshape(tok_rows, heads_here, 2, width_first),
        query_second.reshape(tok_rows, heads_here, 2, width_second),
    )
    key_widths = (width_first, width_second)
    start_state = (
        jnp.full((heads_here, 2, tok_rows, 1), -1e30, jnp.float32),
        jnp.zeros((heads_here, 2, tok_rows, 1), jnp.float32),
        jnp.zeros((heads_here, 2, tok_rows, value_size), jnp.float32),
    )
    states = (start_state, start_state)
    pieces = (
        lax.all_gather(key_first, "sp", axis=0, tiled=True),
        lax.all_gather(key_second, "sp", axis=0, tiled=True),
        lax.all_gather(values, "sp", axis=0, tiled=True),
    )
    piece_rows = pieces[0].shape[0]
    key_pos = lax.broadcasted_iota(jnp.int32, (1, piece_rows), 1)
    allowed = key_pos <= query_pos
    value_rows = pieces[2].reshape(piece_rows, 2, heads_here, value_size)
    results = []
    for group_idx in range(2):
        key_width = key_widths[group_idx]
        key_part = pieces[group_idx].reshape(piece_rows, heads_here, 2, key_width)
        scores = jnp.einsum(
            "qhmd,khmd->hmqk", query_groups[group_idx], key_part, preferred_element_type=jnp.float32
        ) * key_width ** (-0.5)
        scores = jnp.where(allowed, scores, -1e30)
        running, totals, weighted = states[group_idx]
        new_peak = jnp.maximum(running, jnp.max(scores, axis=-1, keepdims=True))
        weights = jnp.where(allowed, jnp.exp(scores - new_peak), 0.0)
        totals = jnp.sum(weights, axis=-1, keepdims=True)
        weighted = jnp.einsum(
            "hmqk,khe->hmqe",
            weights.astype(jnp.bfloat16),
            value_rows[:, group_idx],
            preferred_element_type=jnp.float32,
        )
        results.append((new_peak, totals, weighted))
    states = (results[0], results[1])
    map_out = jnp.stack([states[0][2] / states[0][1], states[1][2] / states[1][1]])
    differ = map_out[:, :, 0] - lambdas[:, :, None, None] * map_out[:, :, 1]
    head_scale = lax.rsqrt(jnp.mean(differ * differ, axis=-1, keepdims=True) + 1e-06)
    attended = (0.8 * differ * head_scale).astype(jnp.bfloat16)
    projection = out_weight.reshape(2, heads_here, value_size, out_weight.shape[2])
    mixed_part = jnp.einsum(
        "ghqe,gher->qr", attended, projection, preferred_element_type=jnp.float32
    )
    mixed = lax.psum_scatter(
        mixed_part.astype(jnp.bfloat16), "tp", scatter_dimension=1, tiled=True
    ).astype(jnp.float32)
    stream = residual.astype(jnp.float32) + mixed
    squares = lax.psum(jnp.sum(stream * stream, axis=1), "tp")
    row_scale = lax.rsqrt(squares[:, None] / D + 1e-06)
    normed = (stream * row_scale * norm_gain.astype(jnp.float32)).astype(jnp.bfloat16)
    full_rows = lax.all_gather(normed, "tp", axis=1, tiled=True)
    pieces = (
        lax.all_gather(gate_weight, "sp", axis=0, tiled=True),
        lax.all_gather(up_weight, "sp", axis=0, tiled=True),
    )
    gate = jnp.dot(full_rows, pieces[0], preferred_element_type=jnp.float32)
    up_part = jnp.dot(full_rows, pieces[1], preferred_element_type=jnp.float32)
    hidden = (jax.nn.silu(gate) * up_part).astype(jnp.bfloat16)
    partial_out = jnp.dot(
        hidden,
        lax.all_gather(down_weight, "sp", axis=1, tiled=True),
        preferred_element_type=jnp.float32,
    )
    ffn = lax.psum_scatter(
        partial_out.astype(jnp.bfloat16), "tp", scatter_dimension=1, tiled=True
    ).astype(jnp.float32)
    return (stream + 0.5 * ffn).astype(jnp.bfloat16)


def solution(mesh):
    return jax.shard_map(
        per_device,
        mesh=mesh,
        in_specs=(
            P(("grp", "sp"), "tp"),
            P(("grp", "sp"), "tp"),
            P(("grp", "sp"), "tp"),
            P(("grp", "sp"), "tp"),
            P(("grp", "sp"), None, "tp"),
            P(None, "tp"),
            P(("grp", "sp"), "tp"),
            P("tp"),
            P(None, "tp", None),
            P("sp", "tp"),
            P("sp", "tp"),
            P("tp", "sp"),
        ),
        out_specs=P(("grp", "sp"), "tp"),
        check_vma=False,
    )
```

profile of v0, /device:TPU:0, one launch (start us, length us, event | category | flops | bytes accessed | tf_op | source)
XLA Modules:
  0.0 419.4 jit_solution(9682786560967322755)
XLA Ops:
  7.4 0.0 copy-start
  7.4 0.0 reduce-scatter.3.cloned.1.call-start
  7.4 0.1 iota_compare_fusion
  7.6 16.6 %all_gather.23 = bf16[768,256]{1,0:T(8,128)(2,1)S(1)} all-gather(bf16[192,256]{1,0:T(8,128)(2,1)} %param.15), channel_id=1, replica_groups=mesh['grp'=2,'sp'=4,'tp'=4] {'sp'}, dimensions={0}, use_global_device_ids=true | all-gather | bytes 491520 | tf_op jit(solution)/shard_map/all_gather | solution.py:43
  24.2 0.2 copy.28
  24.4 0.0 copy-done.6
  24.4 14.4 %all_gather.21 = bf16[768,128]{1,0:T(8,128)(2,1)S(1)} all-gather(bf16[192,128]{1,0:T(8,128)(2,1)S(1)} %copy-done.6), channel_id=1, replica_groups=mesh['grp'=2,'sp'=4,'tp'=4] {'sp'}, dimensions={0}, use_global_device_ids=true | all-gather | bytes 245760 | tf_op jit(solution)/shard_map/all_gather | solution.py:42
  38.8 0.1 copy.26
  38.9 0.0 copy-done.5
  38.9 0.1 copy.25
  39.0 0.0 copy-done.4
  39.1 14.8 %all_gather.22 = bf16[768,2,128]{2,0,1:T(8,128)(2,1)S(1)} all-gather(bf16[192,2,128]{2,0,1:T(8,128)(2,1)S(1)} %copy.27), channel_id=1, replica_groups=mesh['grp'=2,'sp'=4,'tp'=4] {'sp'}, dimensions={0}, use_global_device_ids=true | all-gather | bytes 491520 | tf_op jit(solution)/shard_map/all_gather | solution.py:44
  53.8 0.0 copy-done.3
  53.8 0.5 fusion.34
  54.3 0.5 fusion.35
  54.8 0.7 fusion.6
  55.5 0.4 fusion.5
  55.9 0.0 copy-start.7
  55.9 0.4 fusion.4
  56.4 0.2 copy-done.7
  56.6 0.2 fusion.21
  56.8 0.0 copy-done
  56.8 1.3 fusion
  58.2 0.0 reduce-scatter.3.cloned.1.call-update
  58.2 0.0 all-gather.4.cloned.1.call-start
  58.3 0.5 all-gather.4.cloned.1.call-update
  58.8 0.0 copy-start.8
  58.8 0.0 copy-start.1
  58.8 0.0 all-gather.6.cloned.1.call-start
  58.9 0.5 all-gather.6.cloned.1.call-update
  59.4 0.0 all-gather.8.cloned.1.call-start
  59.4 0.5 all-gather.8.cloned.1.call-update
  60.0 0.0 reduce-scatter.5.cloned.1.call-start
  60.0 0.0 copy-done.8
  60.0 22.8 %reduce-scatter.3.cloned.1.call-done = bf16[192,512]{1,0:T(8,128)(2,1)} async-done(((bf16[192,2048]{1,0:T(8,128)(2,1)}), bf16[192,512]{1,0:T(8,128)(2,1)}) %reduce-scatter.3.cloned.1.call-update) | async-done | bytes 196624 | tf_op jit(solution)/shard_map/reduce_scatter | solution.py:78
  82.8 1.1 multiply_reduce_fusion
  83.9 6.1 %psum.7 = f32[192]{0:T(256)S(1)} all-reduce(f32[192]{0:T(256)S(1)} %multiply_reduce_fusion), channel_id=1, replica_groups=mesh['grp'=2,'sp'=4,'tp'=4] {'tp'}, use_global_device_ids=true, to_apply=%region_7.8 | all-reduce | flops 192 | bytes 1536 | tf_op jit(solution)/shard_map/psum | solution.py:82
  90.0 1.0 multiply_convert_fusion
  91.0 8.4 %all_gather.24 = bf16[192,2048]{1,0:T(8,128)(2,1)S(1)} all-gather(bf16[192,512]{1,0:T(8,128)(2,1)S(1)} %multiply_convert_fusion), channel_id=1, replica_groups=mesh['grp'=2,'sp'=4,'tp'=4] {'tp'}, dimensions={1}, use_global_device_ids=true | all-gather | bytes 983040 | tf_op jit(solution)/shard_map/all_gather | solution.py:85
  99.4 68.7 %all-gather.4.cloned.1.call-done = bf16[2048,1408]{1,0:T(8,128)(2,1)} async-done(((bf16[512,1408]{1,0:T(8,128)(2,1)}), bf16[2048,1408]{1,0:T(8,128)(2,1)}) %all-gather.4.cloned.1.call-update) | async-done | bytes 5767184 | tf_op jit(solution)/shard_map/all_gather | solution.py:87
  168.1 4.0 fusion.36
  172.1 102.2 %all-gather.6.cloned.1.call-done = bf16[2048,1408]{1,0:T(8,128)(2,1)} async-done(((bf16[512,1408]{1,0:T(8,128)(2,1)}), bf16[2048,1408]{1,0:T(8,128)(2,1)}) %all-gather.6.cloned.1.call-update) | async-done | bytes 5767184 | tf_op jit(solution)/shard_map/all_gather | solution.py:88
  274.4 106.3 %all-gather.8.cloned.1.call-done = bf16[1408,2048]{1,0:T(8,128)(2,1)} async-done(((bf16[1408,512]{1,0:T(8,128)(2,1)}), bf16[1408,2048]{1,0:T(8,128)(2,1)}) %all-gather.8.cloned.1.call-update) | async-done | bytes 5767184 | tf_op jit(solution)/shard_map/all_gather | solution.py:95
  380.6 7.9 %convolution_convert_fusion = bf16[192,2048]{1,0:T(8,128)(2,1)} fusion(bf16[1408,2048]{1,0:T(8,128)(2,1)} %all-gather.8.cloned.1.call-done, bf16[192,2048]{1,0:T(8,128)(2,1)S(1)} %all_gather.24, bf16[2048,1408]{1,0:T(8,128)(2,1)} %all-gather.6.cloned.1.call-done, f32[192,1408]{1,0:T(8,128)S(1)} %fusion.36), kind=kOutput, calls=%fused_computation.4 | convolution fusion | flops 2216607744 | bytes 14188544 | tf_op jit(solution)/shard_map/dot_general | solution.py:93
  388.5 0.0 reduce-scatter.5.cloned.1.call-update
  388.5 21.6 %reduce-scatter.5.cloned.1.call-done = bf16[192,512]{1,0:T(8,128)(2,1)} async-done(((bf16[192,2048]{1,0:T(8,128)(2,1)}), bf16[192,512]{1,0:T(8,128)(2,1)}) %reduce-scatter.5.cloned.1.call-update) | async-done | bytes 196624 | tf_op jit(solution)/shard_map/reduce_scatter | solution.py:98
  410.2 0.0 copy-done.2
  410.2 1.7 add_convert_fusion
  (12 shorter events, 0.1 us)
Async XLA Ops:
  7.4 49.5 %copy-start = (bf16[2,128,2048]{2,1,0:T(8,128)(2,1)S(1)}, bf16[2,128,2048]{2,1,0:T(8,128)(2,1)}, u32[]{:S(2)}) copy-start(bf16[2,128,2048]{2,1,0:T(8,128)(2,1)} %param.20) | copy-start | bytes 3145732
  7.4 17.0 %copy-start.6 = (bf16[192,128]{1,0:T(8,128)(2,1)S(1)}, bf16[192,128]{1,0:T(8,128)(2,1)}, u32[]{:S(2)}) copy-start(bf16[192,128]{1,0:T(8,128)(2,1)} %param.13) | copy-start | bytes 147460
  7.4 31.5 %copy-start.5 = (bf16[192,128]{1,0:T(8,128)(2,1)S(1)}, bf16[192,128]{1,0:T(8,128)(2,1)}, u32[]{:S(2)}) copy-start(bf16[192,128]{1,0:T(8,128)(2,1)} %param.12) | copy-start | bytes 147460
  7.4 31.7 %copy-start.4 = (bf16[192,2,128]{2,1,0:T(2,128)(2,1)S(1)}, bf16[192,2,128]{2,1,0:T(2,128)(2,1)}, u32[]{:S(2)}) copy-start(bf16[192,2,128]{2,1,0:T(2,128)(2,1)} %param.16) | copy-start | bytes 294916
  7.4 75.4 %reduce-scatter.3.cloned.1.call-start = ((), (), s32[]{:S(2)}) async-start(), calls=%async_computation.2 | async-start | bytes 983040 | tf_op jit(solution)/shard_map/reduce_scatter | solution.py:78
  24.2 29.6 %copy-start.3 = (bf16[192,256]{1,0:T(8,128)(2,1)S(1)}, bf16[192,256]{1,0:T(8,128)(2,1)}, u32[]{:S(2)}) copy-start(bf16[192,256]{1,0:T(8,128)(2,1)} %param.14) | copy-start | bytes 294916
  55.9 0.7 copy-start.7
  58.2 109.9 %all-gather.4.cloned.1.call-start = ((), (), s32[]{:S(2)}) async-start(), calls=%async_computation.3 | async-start | bytes 7208960 | tf_op jit(solution)/shard_map/all_gather | solution.py:87
  58.8 1.2 copy-start.8
  58.8 24.0 %copy-start.1 = (bf16[192,512]{1,0:T(8,128)(2,1)S(1)}, bf16[192,512]{1,0:T(8,128)(2,1)}, u32[]{:S(2)}) copy-start(bf16[192,512]{1,0:T(8,128)(2,1)} %param.18) | copy-start | bytes 589828
  58.8 215.6 %all-gather.6.cloned.1.call-start = ((), (), s32[]{:S(2)}) async-start(), calls=%async_computation.4 | async-start | bytes 7208960 | tf_op jit(solution)/shard_map/all_gather | solution.py:88
  59.4 321.3 %all-gather.8.cloned.1.call-start = ((), (), s32[]{:S(2)}) async-start(), calls=%async_computation.5 | async-start | bytes 7208960 | tf_op jit(solution)/shard_map/all_gather | solution.py:95
  60.0 350.2 %reduce-scatter.5.cloned.1.call-start = ((), (), s32[]{:S(2)}) async-start(), calls=%async_computation.6 | async-start | bytes 983040 | tf_op jit(solution)/shard_map/reduce_scatter | solution.py:98
  172.1 238.0 %copy-start.2 = (bf16[192,512]{1,0:T(8,128)(2,1)S(1)}, bf16[192,512]{1,0:T(8,128)(2,1)}, u32[]{:S(2)}) copy-start(bf16[192,512]{1,0:T(8,128)(2,1)} %reduce-scatter.3.cloned.1.call-done) | copy-start | bytes 589828
Sparse Core Ops, SparseCore 0:
  58.3 24.4 reduce-scatter.2
  388.7 21.4 reduce-scatter.4
Sparse Core Ops, SparseCore 1:
  60.3 107.8 all-gather.3
  169.5 104.8 all-gather.5
  275.8 104.8 all-gather.7
where the time goes:
time: 420 us; the launch traced here: 419 us
  waiting for transfers between devices  323 us (77%)
  blocking collectives  60.2 us (14%)
  between operations  15.2 us (4%)
  matrix products  15.1 us (4%)
  other arithmetic  4.87 us (1%)
    all_gather x1, waiting for transfers between devices, per_device(): lax.all_gather(down_weight, 'sp', axis=1, tiled=True)  106 us
    all_gather x1, waiting for transfers between devices, per_device(): lax.all_gather(up_weight, 'sp', axis=0, tiled=True)  102 us
    all_gather x1, waiting for transfers between devices, per_device(): lax.all_gather(gate_weight, 'sp', axis=0, tiled=True)  68.7 us
    reduce_scatter x1, waiting for transfers between devices, per_device(): lax.psum_scatter(mixed_part.astype(jnp.bfloat16), 'tp', scatter_dimension...  22.8 us
    reduce_scatter x1, waiting for transfers between devices, per_device(): lax.psum_scatter(partial_out.astype(jnp.bfloat16), 'tp', scatter_dimensio...  21.6 us
    all_gather x1, blocking collectives, per_device(): lax.all_gather(key_second, 'sp', axis=0, tiled=True)  16.6 us
    all_gather x1, blocking collectives, per_device(): lax.all_gather(values, 'sp', axis=0, tiled=True)  14.8 us
    all_gather x1, blocking collectives, per_device(): lax.all_gather(key_first, 'sp', axis=0, tiled=True)  14.4 us
  transfers between devices with their start and end apart: 5, of which 5 were waited for; matrix products, arithmetic and copies ran while one was open for 1% of the time, Pallas kernels for 0%

commit v1 on v0

--- a/solution.py
+++ b/solution.py
@@ -6,7 +6,7 @@
 D = 2048
 
 
-def per_device(
+def gathered_weights(
     query_first,
     key_first,
     query_second,
@@ -101,6 +101,193 @@
     return (stream + 0.5 * ffn).astype(jnp.bfloat16)
 
 
+def shift(array, step, count):
+    return lax.ppermute(array, "sp", [(i, (i + step) % count) for i in range(count)])
+
+
+def swap(array, mask, count):
+    return lax.ppermute(array, "tp", [(i, i ^ mask) for i in range(count)])
+
+
+def swap_masks(count):
+    masks = []
+    while count > 1:
+        count //= 2
+        masks.append(count)
+    return masks
+
+
+def gather_swapped(array, axis, count):
+    order = [0]
+    for mask in swap_masks(count):
+        array = jnp.concatenate([array, swap(array, mask, count)], axis=axis)
+        order = order + [m ^ mask for m in order]
+    return array, order
+
+
+def pick(stack, index):
+    return lax.dynamic_index_in_dim(stack, index, 0, keepdims=False)
+
+
+def exchanged_weights(
+    query_first,
+    key_first,
+    query_second,
+    key_second,
+    values,
+    lambdas,
+    residual,
+    norm_gain,
+    out_weight,
+    gate_weight,
+    up_weight,
+    down_weight,
+):
+    n_sp = lax.axis_size("sp")
+    n_tp = lax.axis_size("tp")
+    s = lax.axis_index("sp")
+    t = lax.axis_index("tp")
+    tok_rows = query_first.shape[0]
+    heads_here = lambdas.shape[1]
+    value_size = values.shape[2] // heads_here
+    model = out_weight.shape[2]
+
+    own_kv = jnp.concatenate(
+        [key_first, key_second, values.reshape(tok_rows, -1)], axis=1
+    )
+    kv_blocks = [own_kv] + [
+        lax.ppermute(own_kv, "sp", [(i, i + d) for i in range(n_sp - d)])
+        for d in range(1, n_sp)
+    ]
+    kv = jnp.concatenate(kv_blocks, axis=0)
+
+    kv, out_weight, residual, gate_weight, up_weight, down_weight = lax.optimization_barrier(
+        (kv, out_weight, residual, gate_weight, up_weight, down_weight)
+    )
+    ow_all, order = gather_swapped(
+        out_weight.reshape(-1, model), 0, n_tp
+    )
+    res_rows = jnp.concatenate(
+        [residual] + [shift(residual, d, n_sp) for d in range(1, n_sp)]
+        + [jnp.broadcast_to(norm_gain[None, :], (16, norm_gain.shape[0]))],
+        axis=0,
+    )
+    all_rows = tok_rows * n_sp
+    res_all, _ = gather_swapped(res_rows[None], 0, n_tp)
+    inverse = jnp.asarray([order.index(m) for m in range(n_tp)], jnp.int32)
+    res_cols = jnp.concatenate(
+        [pick(res_all, inverse[m ^ t]) for m in range(n_tp)], axis=1
+    )
+    residual_all = res_cols[:all_rows]
+    gain_all = res_cols[all_rows : all_rows + 1].astype(jnp.float32)
+
+    hid = gate_weight.shape[1]
+    width = -(-hid // (n_sp * 128)) * 128
+    starts = [min(j * width, hid - width) for j in range(n_sp)]
+    gate_up = jnp.stack(
+        [
+            jnp.concatenate(
+                [gate_weight[:, a : a + width], up_weight[:, a : a + width]], axis=1
+            )
+            for a in starts
+        ]
+    )
+    down = jnp.stack([down_weight[a : a + width] for a in starts])
+    gu_parts = []
+    dn_parts = []
+    for d in range(n_sp):
+        gu = pick(gate_up, (s + d) % n_sp)
+        dn = pick(down, (s + d) % n_sp)
+        gu_parts.append(gu if d == 0 else shift(gu, d, n_sp))
+        dn_parts.append(dn if d == 0 else shift(dn, d, n_sp))
+    gu_stack = jnp.stack(gu_parts)
+    dn_stack = jnp.stack(dn_parts)
+    gu_all = jnp.concatenate(
+        [pick(gu_stack, (s - b) % n_sp) for b in range(n_sp)], axis=0
+    )
+    dn_all = jnp.concatenate(
+        [pick(dn_stack, (s - b) % n_sp) for b in range(n_sp)], axis=1
+    )
+    cols = model // n_tp
+    dn_tp = jnp.stack([dn_all[:, b * cols : (b + 1) * cols] for b in range(n_tp)])
+    dn_rel = jnp.concatenate([pick(dn_tp, m ^ t) for m in order], axis=1)
+
+    q_idx = lax.broadcasted_iota(jnp.int32, (tok_rows, all_rows), 0)
+    k_idx = lax.broadcasted_iota(jnp.int32, (tok_rows, all_rows), 1)
+    allowed = jnp.where(k_idx < tok_rows, k_idx <= q_idx, k_idx < (s + 1) * tok_rows)
+    offset = 0
+    value_start = key_first.shape[1] + key_second.shape[1]
+    value_all = kv[:, value_start:].reshape(all_rows, 2, heads_here, value_size)
+    outs = []
+    for g, query in enumerate((query_first, query_second)):
+        span = query.shape[1]
+        width_g = span // (2 * heads_here)
+        keys = kv[:, offset : offset + span].reshape(all_rows, heads_here, 2, width_g)
+        offset += span
+        scores = jnp.einsum(
+            "qhmd,khmd->hmqk",
+            query.reshape(tok_rows, heads_here, 2, width_g),
+            keys,
+            preferred_element_type=jnp.float32,
+        ) * width_g ** (-0.5)
+        scores = jnp.where(allowed, scores, -1e30)
+        peak = jnp.max(scores, axis=-1, keepdims=True)
+        weights = jnp.where(allowed, jnp.exp(scores - peak), 0.0)
+        totals = jnp.sum(weights, axis=-1, keepdims=True)
+        weighted = jnp.einsum(
+            "hmqk,khe->hmqe",
+            weights.astype(jnp.bfloat16),
+            value_all[:, g],
+            preferred_element_type=jnp.float32,
+        )
+        outs.append(weighted / totals)
+    map_out = jnp.stack(outs)
+    differ = map_out[:, :, 0] - lambdas[:, :, None, None] * map_out[:, :, 1]
+    head_scale = lax.rsqrt(jnp.mean(differ * differ, axis=-1, keepdims=True) + 1e-06)
+    attended = (0.8 * differ * head_scale).astype(jnp.bfloat16)
+    attended = attended.transpose(2, 0, 1, 3).reshape(tok_rows, -1)
+
+    att_rows = jnp.concatenate(
+        [attended] + [shift(attended, d, n_sp) for d in range(1, n_sp)], axis=0
+    )
+    att_all, _ = gather_swapped(att_rows, 1, n_tp)
+    stream = residual_all.astype(jnp.float32) + jnp.dot(
+        att_all, ow_all, preferred_element_type=jnp.float32
+    )
+    row_scale = lax.rsqrt(jnp.mean(stream * stream, axis=1, keepdims=True) + 1e-06)
+    normed = (stream * row_scale * gain_all).astype(jnp.bfloat16)
+    own_stream = lax.dynamic_slice(stream[:tok_rows], (0, t * cols), (tok_rows, cols))
+
+    unit = lax.broadcasted_iota(jnp.int32, (1, width), 1)
+    first_new = s * width - jnp.minimum(s * width, hid - width)
+    fresh = unit >= first_new
+    total = None
+    for d in list(range(1, n_sp)) + [0]:
+        both = jnp.dot(
+            normed[d * tok_rows : (d + 1) * tok_rows], gu_all,
+            preferred_element_type=jnp.float32,
+        )
+        hidden = jax.nn.silu(both[:, :width]) * both[:, width:]
+        hidden = jnp.where(fresh, hidden, 0.0).astype(jnp.bfloat16)
+        part = jnp.dot(hidden, dn_rel, preferred_element_type=jnp.float32)
+        for mask in reversed(swap_masks(n_tp)):
+            half = part.shape[1] // 2
+            part = part[:, :half] + swap(
+                part[:, half:].astype(jnp.bfloat16), mask, n_tp
+            ).astype(jnp.float32)
+        if d > 0:
+            part = shift(part.astype(jnp.bfloat16), -d, n_sp).astype(jnp.float32)
+        total = part if total is None else total + part
+    return (own_stream + 0.5 * total).astype(jnp.bfloat16)
+
+
+def per_device(*arrays):
+    all_rows = arrays[0].shape[0] * lax.axis_size("sp")
+    if all_rows < arrays[9].shape[1]:
+        return exchanged_weights(*arrays)
+    return gathered_weights(*arrays)
+
+
 def solution(mesh):
     return jax.shard_map(
         per_device,

time: 420 us -> 235 us (0.56)
  waiting for transfers between devices: 323 us -> 147 us
  blocking collectives: 60.2 us -> 0 us
  starting transfers between devices: 0.2 us -> 49.6 us
  local copies, waits for them, and re-layouts: 0.68 us -> 10.9 us
  between operations: 15.2 us -> 8.49 us
    all_gather x3 -> x0, waiting for transfers between devices: 277 us -> none  [the longest x1 106 us: per_device(): lax.all_gather(down_weight, 'sp', axis=1, tiled=True)]
    ppermute x0 -> x32, waiting for transfers between devices: none -> 147 us  [the longest x15 101 us: shift(): lax.ppermute(array, 'sp', [(i, (i + step) % count) for i in range(count)])]
    all_gather x4 -> x0, blocking collectives: 54.1 us -> none  [the longest x1 16.6 us: per_device(): lax.all_gather(key_second, 'sp', axis=0, tiled=True)]
    ppermute x0 -> x32, starting transfers between devices: none -> 49.6 us  [the longest x15 28.7 us: shift(): lax.ppermute(array, 'sp', [(i, (i + step) % count) for i in range(count)])]
    reduce_scatter x2 -> x0, waiting for transfers between devices: 44.4 us -> none  [the longest x1 22.8 us: per_device(): lax.psum_scatter(mixed_part.astype(jnp.bfloat16), 'tp', scatter_dimension...]
    psum x1 -> x0, blocking collectives: 6.06 us -> none  [per_device(): squares = lax.psum(jnp.sum(stream * stream, axis=1), 'tp')]
    unnamed x20 -> x32, local copies, waits for them, and re-layouts: 0.37 us -> 5.97 us
    dot_general x7 -> x11, matrix products: 15.1 us -> 10.9 us  [the longest x1 3.69 us: exchanged_weights(): jnp.dot(att_all, ow_all, preferred_element_type=jnp.float32)]
  transfers between devices with their start and end apart: 5 -> 32, of which waited for: 5 -> 14; matrix products, arithmetic and copies ran while one was open for 1% -> 5% of each run, Pallas kernels for 0% -> 0%
where the time goes in v1:
time: 235 us
  waiting for transfers between devices  147 us (63%)
  starting transfers between devices  49.6 us (21%)
  matrix products  13.3 us (6%)
  local copies, waits for them, and re-layouts  10.9 us (5%)
  between operations  8.49 us (4%)
  other arithmetic  5.86 us (2%)
    ppermute x15, waiting for transfers between devices, shift(): lax.ppermute(array, 'sp', [(i, (i + step) % count) for i in range(count)])  101 us
    ppermute x14, waiting for transfers between devices, swap(): return lax.ppermute(array, 'tp', [(i, i ^ mask) for i in range(count)])  39.1 us
    ppermute x15, starting transfers between devices, shift(): lax.ppermute(array, 'sp', [(i, (i + step) % count) for i in range(count)])  28.7 us
    ppermute x3, starting transfers between devices, exchanged_weights(): lax.ppermute(own_kv, 'sp', [(i, i + d) for i in range(n_sp - d)])  10.8 us
    ppermute x14, starting transfers between devices, swap(): return lax.ppermute(array, 'tp', [(i, i ^ mask) for i in range(count)])  10.2 us
    ppermute x3, waiting for transfers between devices, exchanged_weights(): lax.ppermute(own_kv, 'sp', [(i, i + d) for i in range(n_sp - d)])  7.05 us
    unnamed x32, local copies, waits for them, and re-layouts  5.97 us
  transfers between devices with their start and end apart: 32, of which 14 were waited for; matrix products, arithmetic and copies ran while one was open for 5% of the time, Pallas kernels for 0%

profile of v1, /device:TPU:0, one launch (start us, length us, event | category | flops | bytes accessed | tf_op | source)
XLA Modules:
  0.0 234.8 jit_solution(15470176046675404336)
XLA Ops:
  0.0 0.9 copy.19
  0.9 1.0 copy.20
  1.9 1.0 copy.18
  3.0 7.0 %collective-permute-start.2 = (bf16[192,640]{0,1:T(8,128)(2,1)S(1)}, bf16[192,640]{0,1:T(8,128)(2,1)S(1)}, u32[]{:S(2)}, u32[]{:S(2)}) collective-permute-start(bf16[192,640]{0,1:T(8,128)(2,1)S(1)} %pad_maximum_fusion.13), channel_id=1, source_target_pairs={{0,12},{1,13},{2,14},{3,15},{16,28},{17,29},{18,30},{19,31}} | collective-permute-start | bytes 737288 | tf_op jit(solution)/shard_map/ppermute | solution.py:159
  10.0 1.3 collective-permute-start.1
  11.3 2.5 %collective-permute-start = (bf16[192,640]{0,1:T(8,128)(2,1)S(1)}, bf16[192,640]{0,1:T(8,128)(2,1)S(1)}, u32[]{:S(2)}, u32[]{:S(2)}) collective-permute-start(bf16[192,640]{0,1:T(8,128)(2,1)S(1)} %pad_maximum_fusion.13), channel_id=1, source_target_pairs={{0,4},{4,8},{8,12},{1,5},{5,9},{9,13},{2,6},{6,10},{10,14},{3,7},{... | collective-permute-start | bytes 737288 | tf_op jit(solution)/shard_map/ppermute | solution.py:159
  14.0 1.5 fusion.104
  20.5 0.9 copy.21
  24.0 1.2 collective-permute-done.1
  25.2 5.9 %collective-permute-done = bf16[192,640]{0,1:T(8,128)(2,1)S(1)} collective-permute-done((bf16[192,640]{0,1:T(8,128)(2,1)S(1)}, bf16[192,640]{0,1:T(8,128)(2,1)S(1)}, u32[]{:S(2)}, u32[]{:S(2)}) %collective-permute-start) | collective-permute-done | bytes 245792 | tf_op jit(solution)/shard_map/ppermute | solution.py:159
  31.6 1.5 fusion.105
  33.1 0.8 fusion.108
  33.9 1.4 fusion.25
  36.1 4.4 %collective-permute-start.10 = (bf16[192,256]{1,0:T(8,128)(2,1)S(1)}, bf16[192,256]{1,0:T(8,128)(2,1)S(1)}, u32[]{:S(2)}, u32[]{:S(2)}) collective-permute-start(bf16[192,256]{1,0:T(8,128)(2,1)S(1)} %bitcast.170), channel_id=1, source_target_pairs={{0,12},{4,0},{8,4},{12,8},{1,13},{5,1},{9,5},{13,9},{2,14},{6,2},{... | collective-permute-start | bytes 294920 | tf_op jit(solution)/shard_map/ppermute | solution.py:105
  40.5 6.1 %collective-permute-start.9 = (bf16[192,256]{1,0:T(8,128)(2,1)S(1)}, bf16[192,256]{1,0:T(8,128)(2,1)S(1)}, u32[]{:S(2)}, u32[]{:S(2)}) collective-permute-start(bf16[192,256]{1,0:T(8,128)(2,1)S(1)} %bitcast.171), channel_id=1, source_target_pairs={{0,8},{4,12},{8,0},{12,4},{1,9},{5,13},{9,1},{13,5},{2,10},{6,14},... | collective-permute-start | bytes 294920 | tf_op jit(solution)/shard_map/ppermute | solution.py:105
  46.6 1.9 collective-permute-start.8
  48.6 2.4 %collective-permute-start.3 = (bf16[192,512]{1,0:T(8,128)(2,1)S(1)}, bf16[192,512]{1,0:T(8,128)(2,1)S(1)}, u32[]{:S(2)}, u32[]{:S(2)}) collective-permute-start(bf16[192,512]{1,0:T(8,128)(2,1)S(1)} %copy-done.7), channel_id=1, source_target_pairs={{0,4},{4,8},{8,12},{12,0},{1,5},{5,9},{9,13},{13,1},{2,6},{6,10},{... | collective-permute-start | bytes 589832 | tf_op jit(solution)/shard_map/ppermute | solution.py:105
  52.0 11.4 %collective-permute-done.3 = bf16[192,512]{1,0:T(8,128)(2,1)S(1)} collective-permute-done((bf16[192,512]{1,0:T(8,128)(2,1)S(1)}, bf16[192,512]{1,0:T(8,128)(2,1)S(1)}, u32[]{:S(2)}, u32[]{:S(2)}) %collective-permute-start.3) | collective-permute-done | bytes 196640 | tf_op jit(solution)/shard_map/ppermute | solution.py:105
  63.5 5.0 %collective-permute-done.4 = bf16[192,512]{1,0:T(8,128)(2,1)S(1)} collective-permute-done((bf16[192,512]{1,0:T(8,128)(2,1)S(1)}, bf16[192,512]{1,0:T(8,128)(2,1)S(1)}, u32[]{:S(2)}, u32[]{:S(2)}) %collective-permute-start.4) | collective-permute-done | bytes 196640 | tf_op jit(solution)/shard_map/ppermute | solution.py:105
  68.5 1.5 collective-permute-start.13
  70.0 6.5 %collective-permute-done.5 = bf16[192,512]{1,0:T(8,128)(2,1)S(1)} collective-permute-done((bf16[192,512]{1,0:T(8,128)(2,1)S(1)}, bf16[192,512]{1,0:T(8,128)(2,1)S(1)}, u32[]{:S(2)}, u32[]{:S(2)}) %collective-permute-start.5) | collective-permute-done | bytes 196640 | tf_op jit(solution)/shard_map/ppermute | solution.py:105
  76.5 1.6 collective-permute-start.6
  78.7 2.7 %collective-permute-start.20 = (bf16[384,512]{1,0:T(8,128)(2,1)S(1)}, bf16[384,512]{1,0:T(8,128)(2,1)S(1)}, u32[]{:S(2)}, u32[]{:S(2)}) collective-permute-start(bf16[384,512]{1,0:T(8,128)(2,1)S(1)} %get-tuple-element.40), channel_id=1, source_target_pairs={{0,12},{4,0},{8,4},{12,8},{1,13},{5,1},{9,5},{13,9},{2,14},{6,2},{... | collective-permute-start | bytes 1179656 | tf_op jit(solution)/shard_map/ppermute | solution.py:105
  81.4 1.4 collective-permute-start.19
  82.8 1.8 collective-permute-start.18
  84.6 25.6 %collective-permute-done.6 = bf16[1,784,512]{2,1,0:T(8,128)(2,1)S(1)} collective-permute-done((bf16[1,784,512]{2,1,0:T(8,128)(2,1)S(1)}, bf16[1,784,512]{2,1,0:T(8,128)(2,1)S(1)}, u32[]{:S(2)}, u32[]{:S(2)}) %collective-permute-start.6) | collective-permute-done | bytes 802848 | tf_op jit(solution)/shard_map/ppermute | solution.py:109
  110.2 1.5 collective-permute-start.11
  112.1 4.0 %collective-permute-done.19 = bf16[384,512]{1,0:T(8,128)(2,1)S(1)} collective-permute-done((bf16[384,512]{1,0:T(8,128)(2,1)S(1)}, bf16[384,512]{1,0:T(8,128)(2,1)S(1)}, u32[]{:S(2)}, u32[]{:S(2)}) %collective-permute-start.19) | collective-permute-done | bytes 393248 | tf_op jit(solution)/shard_map/ppermute | solution.py:105
  116.2 2.7 %collective-permute-start.17 = (bf16[512,768]{1,0:T(8,128)(2,1)S(1)}, bf16[512,768]{1,0:T(8,128)(2,1)S(1)}, u32[]{:S(2)}, u32[]{:S(2)}) collective-permute-start(bf16[512,768]{1,0:T(8,128)(2,1)S(1)} %get-tuple-element.28), channel_id=1, source_target_pairs={{0,12},{4,0},{8,4},{12,8},{1,13},{5,1},{9,5},{13,9},{2,14},{6,2},{... | collective-permute-start | bytes 2359304 | tf_op jit(solution)/shard_map/ppermute | solution.py:105
  118.9 0.8 collective-permute-start.15
  120.8 16.1 %collective-permute-done.17 = bf16[512,768]{1,0:T(8,128)(2,1)S(1)} collective-permute-done((bf16[512,768]{1,0:T(8,128)(2,1)S(1)}, bf16[512,768]{1,0:T(8,128)(2,1)S(1)}, u32[]{:S(2)}, u32[]{:S(2)}) %collective-permute-start.17) | collective-permute-done | bytes 786464 | tf_op jit(solution)/shard_map/ppermute | solution.py:105
  136.9 49.5 %collective-permute-done.16 = bf16[512,768]{1,0:T(8,128)(2,1)S(1)} collective-permute-done((bf16[512,768]{1,0:T(8,128)(2,1)S(1)}, bf16[512,768]{1,0:T(8,128)(2,1)S(1)}, u32[]{:S(2)}, u32[]{:S(2)}) %collective-permute-start.16) | collective-permute-done | bytes 786464 | tf_op jit(solution)/shard_map/ppermute | solution.py:105
  188.2 3.7 %multiply_reduce_fusion = (f32[768]{0:T(1024)S(1)}, f32[768,2048]{1,0:T(8,128)S(1)}) fusion(bf16[512,2048]{1,0:T(8,128)(2,1)S(1)} %collective-permute-done.14, bf16[256,2048]{1,0:T(8,128)(2,1)S(1)} %collective-permute-done.13, bf16[256,2048]{1,0:T(8,128)(2,1)S(1)} %bitcast.157, bf16[768,512]{1,0:T(8,128)(2,1)S(1)} %collective-permute-done.12, ...), kind=kOutput, calls=%fused_computation.3 | convolution fusion | flops 3244817664 | bytes 15207424 | tf_op jit(solution)/shard_map/dot_general | solution.py:254
  192.6 2.0 copy-done.2
  194.6 0.8 fusion.31
  195.4 0.8 fusion.29
  196.2 0.8 fusion.27
  197.0 0.8 fusion.33
  202.5 1.5 collective-permute-start.31
  205.0 1.5 collective-permute-start.25
  206.5 3.0 %collective-permute-done.22 = bf16[192,512]{1,0:T(8,128)(2,1)S(1)} collective-permute-done((bf16[192,512]{1,0:T(8,128)(2,1)S(1)}, bf16[192,512]{1,0:T(8,128)(2,1)S(1)}, u32[]{:S(2)}, u32[]{:S(2)}) %collective-permute-start.22) | collective-permute-done | bytes 196640 | tf_op jit(solution)/shard_map/ppermute | solution.py:109
  209.7 8.3 %collective-permute-done.28 = bf16[192,512]{1,0:T(8,128)(2,1)S(1)} collective-permute-done((bf16[192,512]{1,0:T(8,128)(2,1)S(1)}, bf16[192,512]{1,0:T(8,128)(2,1)S(1)}, u32[]{:S(2)}, u32[]{:S(2)}) %collective-permute-start.28) | collective-permute-done | bytes 196640 | tf_op jit(solution)/shard_map/ppermute | solution.py:109
  218.1 1.2 collective-permute-start.29
  219.2 2.1 collective-permute-done.25
  221.4 3.1 %collective-permute-start.26 = (bf16[192,512]{1,0:T(8,128)(2,1)S(1)}, bf16[192,512]{1,0:T(8,128)(2,1)S(1)}, u32[]{:S(2)}, u32[]{:S(2)}) collective-permute-start(bf16[192,512]{1,0:T(8,128)(2,1)S(1)} %fusion.43), channel_id=1, source_target_pairs={{0,8},{4,12},{8,0},{12,4},{1,9},{5,13},{9,1},{13,5},{2,10},{6,14},... | collective-permute-start | bytes 589832 | tf_op jit(solution)/shard_map/ppermute | solution.py:105
  224.5 1.5 slice.213
  226.5 7.5 %collective-permute-done.26 = bf16[192,512]{1,0:T(8,128)(2,1)S(1)} collective-permute-done((bf16[192,512]{1,0:T(8,128)(2,1)S(1)}, bf16[192,512]{1,0:T(8,128)(2,1)S(1)}, u32[]{:S(2)}, u32[]{:S(2)}) %collective-permute-start.26) | collective-permute-done | bytes 196640 | tf_op jit(solution)/shard_map/ppermute | solution.py:105
  234.0 0.8 fusion.41
  (117 shorter events, 13.0 us)
Async XLA Ops:
  0.0 31.6 %copy-start = (bf16[192,256]{1,0:T(8,128)(2,1)S(1)}, bf16[192,256]{1,0:T(8,128)(2,1)}, u32[]{:S(2)}) copy-start(bf16[192,256]{1,0:T(8,128)(2,1)} %param.15) | copy-start | bytes 294916
  3.0 21.0 %collective-permute-start.2 = (bf16[192,640]{0,1:T(8,128)(2,1)S(1)}, bf16[192,640]{0,1:T(8,128)(2,1)S(1)}, u32[]{:S(2)}, u32[]{:S(2)}) collective-permute-start(bf16[192,640]{0,1:T(8,128)(2,1)S(1)} %pad_maximum_fusion.13), channel_id=1, source_target_pairs={{0,12},{1,13},{2,14},{3,15},{16,28},{17,29},{18,30},{19,31}} | collective-permute-start | bytes 737288 | tf_op jit(solution)/shard_map/ppermute | solution.py:159
  10.0 15.2 %collective-permute-start.1 = (bf16[192,640]{0,1:T(8,128)(2,1)S(1)}, bf16[192,640]{0,1:T(8,128)(2,1)S(1)}, u32[]{:S(2)}, u32[]{:S(2)}) collective-permute-start(bf16[192,640]{0,1:T(8,128)(2,1)S(1)} %pad_maximum_fusion.13), channel_id=1, source_target_pairs={{0,8},{4,12},{1,9},{5,13},{2,10},{6,14},{3,11},{7,15},{16,24},{20,... | collective-permute-start | bytes 737288 | tf_op jit(solution)/shard_map/ppermute | solution.py:159
  11.3 19.7 %collective-permute-start = (bf16[192,640]{0,1:T(8,128)(2,1)S(1)}, bf16[192,640]{0,1:T(8,128)(2,1)S(1)}, u32[]{:S(2)}, u32[]{:S(2)}) collective-permute-start(bf16[192,640]{0,1:T(8,128)(2,1)S(1)} %pad_maximum_fusion.13), channel_id=1, source_target_pairs={{0,4},{4,8},{8,12},{1,5},{5,9},{9,13},{2,6},{6,10},{10,14},{3,7},{... | collective-permute-start | bytes 737288 | tf_op jit(solution)/shard_map/ppermute | solution.py:159
  33.0 2.6 %copy-start.9 = (f32[2,1]{0,1:T(1,128)S(1)}, f32[2,1]{0,1:T(1,128)}, u32[]{:S(2)}) copy-start(f32[2,1]{0,1:T(1,128)} %param.18) | copy-start | bytes 28
  33.0 15.5 %copy-start.7 = (bf16[192,512]{1,0:T(8,128)(2,1)S(1)}, bf16[192,512]{1,0:T(8,128)(2,1)}, u32[]{:S(2)}) copy-start(bf16[192,512]{1,0:T(8,128)(2,1)} %param.19) | copy-start | bytes 589828
  33.1 18.0 %copy-start.3 = (bf16[1408,512]{1,0:T(8,128)(2,1)S(1)}, bf16[1408,512]{1,0:T(8,128)(2,1)}, u32[]{:S(2)}) copy-start(bf16[1408,512]{1,0:T(8,128)(2,1)} %param.24) | copy-start | bytes 4325380
  35.3 15.9 %copy-start.4 = (bf16[512,1408]{1,0:T(8,128)(2,1)S(1)}, bf16[512,1408]{1,0:T(8,128)(2,1)}, u32[]{:S(2)}) copy-start(bf16[512,1408]{1,0:T(8,128)(2,1)} %param.22) | copy-start | bytes 4325380
  35.3 15.9 %copy-start.5 = (bf16[512,1408]{1,0:T(8,128)(2,1)S(1)}, bf16[512,1408]{1,0:T(8,128)(2,1)}, u32[]{:S(2)}) copy-start(bf16[512,1408]{1,0:T(8,128)(2,1)} %param.23) | copy-start | bytes 4325380
  36.1 46.7 %collective-permute-start.10 = (bf16[192,256]{1,0:T(8,128)(2,1)S(1)}, bf16[192,256]{1,0:T(8,128)(2,1)S(1)}, u32[]{:S(2)}, u32[]{:S(2)}) collective-permute-start(bf16[192,256]{1,0:T(8,128)(2,1)S(1)} %bitcast.170), channel_id=1, source_target_pairs={{0,12},{4,0},{8,4},{12,8},{1,13},{5,1},{9,5},{13,9},{2,14},{6,2},{... | collective-permute-start | bytes 294920 | tf_op jit(solution)/shard_map/ppermute | solution.py:105
  40.5 40.9 %collective-permute-start.9 = (bf16[192,256]{1,0:T(8,128)(2,1)S(1)}, bf16[192,256]{1,0:T(8,128)(2,1)S(1)}, u32[]{:S(2)}, u32[]{:S(2)}) collective-permute-start(bf16[192,256]{1,0:T(8,128)(2,1)S(1)} %bitcast.171), channel_id=1, source_target_pairs={{0,8},{4,12},{8,0},{12,4},{1,9},{5,13},{9,1},{13,5},{2,10},{6,14},... | collective-permute-start | bytes 294920 | tf_op jit(solution)/shard_map/ppermute | solution.py:105
  46.6 32.1 %collective-permute-start.8 = (bf16[192,256]{1,0:T(8,128)(2,1)S(1)}, bf16[192,256]{1,0:T(8,128)(2,1)S(1)}, u32[]{:S(2)}, u32[]{:S(2)}) collective-permute-start(bf16[192,256]{1,0:T(8,128)(2,1)S(1)} %bitcast.172), channel_id=1, source_target_pairs={{0,4},{4,8},{8,12},{12,0},{1,5},{5,9},{9,13},{13,1},{2,6},{6,10},{... | collective-permute-start | bytes 294920 | tf_op jit(solution)/shard_map/ppermute | solution.py:105
  48.6 19.9 %collective-permute-start.4 = (bf16[192,512]{1,0:T(8,128)(2,1)S(1)}, bf16[192,512]{1,0:T(8,128)(2,1)S(1)}, u32[]{:S(2)}, u32[]{:S(2)}) collective-permute-start(bf16[192,512]{1,0:T(8,128)(2,1)S(1)} %copy-done.7), channel_id=1, source_target_pairs={{0,8},{4,12},{8,0},{12,4},{1,9},{5,13},{9,1},{13,5},{2,10},{6,14},... | collective-permute-start | bytes 589832 | tf_op jit(solution)/shard_map/ppermute | solution.py:105
  48.6 14.9 %collective-permute-start.3 = (bf16[192,512]{1,0:T(8,128)(2,1)S(1)}, bf16[192,512]{1,0:T(8,128)(2,1)S(1)}, u32[]{:S(2)}, u32[]{:S(2)}) collective-permute-start(bf16[192,512]{1,0:T(8,128)(2,1)S(1)} %copy-done.7), channel_id=1, source_target_pairs={{0,4},{4,8},{8,12},{12,0},{1,5},{5,9},{9,13},{13,1},{2,6},{6,10},{... | collective-permute-start | bytes 589832 | tf_op jit(solution)/shard_map/ppermute | solution.py:105
  51.7 16.8 %copy-start.6 = (bf16[2,128,2048]{2,1,0:T(8,128)(2,1)S(1)}, bf16[2,128,2048]{2,1,0:T(8,128)(2,1)}, u32[]{:S(2)}) copy-start(bf16[2,128,2048]{2,1,0:T(8,128)(2,1)} %param.21) | copy-start | bytes 3145732
  51.7 24.8 %copy-start.8 = (bf16[512]{0:T(512)(128)(2,1)S(1)}, bf16[512]{0:T(512)(128)(2,1)}, u32[]{:S(2)}) copy-start(bf16[512]{0:T(512)(128)(2,1)} %param.20) | copy-start | bytes 3076
  63.4 13.0 %collective-permute-start.5 = (bf16[192,512]{1,0:T(8,128)(2,1)S(1)}, bf16[192,512]{1,0:T(8,128)(2,1)S(1)}, u32[]{:S(2)}, u32[]{:S(2)}) collective-permute-start(bf16[192,512]{1,0:T(8,128)(2,1)S(1)} %copy-done.7), channel_id=1, source_target_pairs={{0,12},{4,0},{8,4},{12,8},{1,13},{5,1},{9,5},{13,9},{2,14},{6,2},{... | collective-permute-start | bytes 589832 | tf_op jit(solution)/shard_map/ppermute | solution.py:105
  68.5 50.4 %collective-permute-start.13 = (bf16[256,2048]{1,0:T(8,128)(2,1)S(1)}, bf16[256,2048]{1,0:T(8,128)(2,1)S(1)}, u32[]{:S(2)}, u32[]{:S(2)}) collective-permute-start(bf16[256,2048]{1,0:T(8,128)(2,1)S(1)} %bitcast.155), channel_id=1, source_target_pairs={{0,2},{1,3},{2,0},{3,1},{4,6},{5,7},{6,4},{7,5},{8,10},{9,11},{10,... | collective-permute-start | bytes 3145736 | tf_op jit(solution)/shard_map/ppermute | solution.py:109
  76.5 33.7 %collective-permute-start.6 = (bf16[1,784,512]{2,1,0:T(8,128)(2,1)S(1)}, bf16[1,784,512]{2,1,0:T(8,128)(2,1)S(1)}, u32[]{:S(2)}, u32[]{:S(2)}) collective-permute-start(bf16[1,784,512]{2,1,0:T(8,128)(2,1)S(1)} %bitcast.150), channel_id=1, source_target_pairs={{0,2},{1,3},{2,0},{3,1},{4,6},{5,7},{6,4},{7,5},{8,10},{9,11},{10,... | collective-permute-start | bytes 2408456 | tf_op jit(solution)/shard_map/ppermute | solution.py:109
  78.7 33.1 %collective-permute-start.20 = (bf16[384,512]{1,0:T(8,128)(2,1)S(1)}, bf16[384,512]{1,0:T(8,128)(2,1)S(1)}, u32[]{:S(2)}, u32[]{:S(2)}) collective-permute-start(bf16[384,512]{1,0:T(8,128)(2,1)S(1)} %get-tuple-element.40), channel_id=1, source_target_pairs={{0,12},{4,0},{8,4},{12,8},{1,13},{5,1},{9,5},{13,9},{2,14},{6,2},{... | collective-permute-start | bytes 1179656 | tf_op jit(solution)/shard_map/ppermute | solution.py:105
  81.4 34.7 %collective-permute-start.19 = (bf16[384,512]{1,0:T(8,128)(2,1)S(1)}, bf16[384,512]{1,0:T(8,128)(2,1)S(1)}, u32[]{:S(2)}, u32[]{:S(2)}) collective-permute-start(bf16[384,512]{1,0:T(8,128)(2,1)S(1)} %get-tuple-element.41), channel_id=1, source_target_pairs={{0,8},{4,12},{8,0},{12,4},{1,9},{5,13},{9,1},{13,5},{2,10},{6,14},... | collective-permute-start | bytes 1179656 | tf_op jit(solution)/shard_map/ppermute | solution.py:105
  82.8 36.1 %collective-permute-start.18 = (bf16[384,512]{1,0:T(8,128)(2,1)S(1)}, bf16[384,512]{1,0:T(8,128)(2,1)S(1)}, u32[]{:S(2)}, u32[]{:S(2)}) collective-permute-start(bf16[384,512]{1,0:T(8,128)(2,1)S(1)} %get-tuple-element.42), channel_id=1, source_target_pairs={{0,4},{4,8},{8,12},{12,0},{1,5},{5,9},{9,13},{13,1},{2,6},{6,10},{... | collective-permute-start | bytes 1179656 | tf_op jit(solution)/shard_map/ppermute | solution.py:105
  110.2 9.8 %collective-permute-start.11 = (bf16[768,256]{1,0:T(8,128)(2,1)S(1)}, bf16[768,256]{1,0:T(8,128)(2,1)S(1)}, u32[]{:S(2)}, u32[]{:S(2)}) collective-permute-start(bf16[768,256]{1,0:T(8,128)(2,1)S(1)} %constant_dynamic-update-slice_fusion.5), channel_id=1, source_target_pairs={{0,2},{1,3},{2,0},{3,1},{4,6},{5,7},{6,4},{7,5},{8,10},{9,11},{10,... | collective-permute-start | bytes 1179656 | tf_op jit(solution)/shard_map/ppermute | solution.py:109
  111.8 75.3 %collective-permute-start.7 = (bf16[2,784,512]{2,1,0:T(8,128)(2,1)S(1)}, bf16[2,784,512]{2,1,0:T(8,128)(2,1)S(1)}, u32[]{:S(2)}, u32[]{:S(2)}) collective-permute-start(bf16[2,784,512]{2,1,0:T(8,128)(2,1)S(1)} %pad_maximum_fusion.6), channel_id=1, source_target_pairs={{0,1},{1,0},{2,3},{3,2},{4,5},{5,4},{6,7},{7,6},{8,9},{9,8},{10,11... | collective-permute-start | bytes 4816904 | tf_op jit(solution)/shard_map/ppermute | solution.py:109
  116.2 20.8 %collective-permute-start.17 = (bf16[512,768]{1,0:T(8,128)(2,1)S(1)}, bf16[512,768]{1,0:T(8,128)(2,1)S(1)}, u32[]{:S(2)}, u32[]{:S(2)}) collective-permute-start(bf16[512,768]{1,0:T(8,128)(2,1)S(1)} %get-tuple-element.28), channel_id=1, source_target_pairs={{0,12},{4,0},{8,4},{12,8},{1,13},{5,1},{9,5},{13,9},{2,14},{6,2},{... | collective-permute-start | bytes 2359304 | tf_op jit(solution)/shard_map/ppermute | solution.py:105
  118.9 67.6 %collective-permute-start.16 = (bf16[512,768]{1,0:T(8,128)(2,1)S(1)}, bf16[512,768]{1,0:T(8,128)(2,1)S(1)}, u32[]{:S(2)}, u32[]{:S(2)}) collective-permute-start(bf16[512,768]{1,0:T(8,128)(2,1)S(1)} %get-tuple-element.29), channel_id=1, source_target_pairs={{0,8},{4,12},{8,0},{12,4},{1,9},{5,13},{9,1},{13,5},{2,10},{6,14},... | collective-permute-start | bytes 2359304 | tf_op jit(solution)/shard_map/ppermute | solution.py:105
  118.9 67.6 %collective-permute-start.15 = (bf16[512,768]{1,0:T(8,128)(2,1)S(1)}, bf16[512,768]{1,0:T(8,128)(2,1)S(1)}, u32[]{:S(2)}, u32[]{:S(2)}) collective-permute-start(bf16[512,768]{1,0:T(8,128)(2,1)S(1)} %get-tuple-element.30), channel_id=1, source_target_pairs={{0,4},{4,8},{8,12},{12,0},{1,5},{5,9},{9,13},{13,1},{2,6},{6,10},{... | collective-permute-start | bytes 2359304 | tf_op jit(solution)/shard_map/ppermute | solution.py:105
  120.0 68.2 %collective-permute-start.14 = (bf16[512,2048]{1,0:T(8,128)(2,1)S(1)}, bf16[512,2048]{1,0:T(8,128)(2,1)S(1)}, u32[]{:S(2)}, u32[]{:S(2)}) collective-permute-start(bf16[512,2048]{1,0:T(8,128)(2,1)S(1)} %pad_maximum_fusion.5), channel_id=1, source_target_pairs={{0,1},{1,0},{2,3},{3,2},{4,5},{5,4},{6,7},{7,6},{8,9},{9,8},{10,11... | collective-permute-start | bytes 6291464 | tf_op jit(solution)/shard_map/ppermute | solution.py:109
  136.9 51.3 %collective-permute-start.12 = (bf16[768,512]{1,0:T(8,128)(2,1)S(1)}, bf16[768,512]{1,0:T(8,128)(2,1)S(1)}, u32[]{:S(2)}, u32[]{:S(2)}) collective-permute-start(bf16[768,512]{1,0:T(8,128)(2,1)S(1)} %pad_maximum_fusion.12), channel_id=1, source_target_pairs={{0,1},{1,0},{2,3},{3,2},{4,5},{5,4},{6,7},{7,6},{8,9},{9,8},{10,11... | collective-permute-start | bytes 2359304 | tf_op jit(solution)/shard_map/ppermute | solution.py:109
  191.9 2.6 %copy-start.2 = (f32[768,2048]{1,0:T(8,128)}, f32[768,2048]{1,0:T(8,128)S(1)}, u32[]{:S(2)}) copy-start(f32[768,2048]{1,0:T(8,128)S(1)} %get-tuple-element.66) | copy-start | bytes 18874372
  198.4 3.2 %collective-permute-start.21 = (bf16[192,1024]{1,0:T(8,128)(2,1)S(1)}, bf16[192,1024]{1,0:T(8,128)(2,1)S(1)}, u32[]{:S(2)}, u32[]{:S(2)}) collective-permute-start(bf16[192,1024]{1,0:T(8,128)(2,1)S(1)} %slice.334), channel_id=1, source_target_pairs={{0,1},{1,0},{2,3},{3,2},{4,5},{5,4},{6,7},{7,6},{8,9},{9,8},{10,11... | collective-permute-start | bytes 1179656 | tf_op jit(solution)/shard_map/ppermute | solution.py:109
  199.2 3.2 %collective-permute-start.30 = (bf16[192,1024]{1,0:T(8,128)(2,1)S(1)}, bf16[192,1024]{1,0:T(8,128)(2,1)S(1)}, u32[]{:S(2)}, u32[]{:S(2)}) collective-permute-start(bf16[192,1024]{1,0:T(8,128)(2,1)S(1)} %slice.331), channel_id=1, source_target_pairs={{0,1},{1,0},{2,3},{3,2},{4,5},{5,4},{6,7},{7,6},{8,9},{9,8},{10,11... | collective-permute-start | bytes 1179656 | tf_op jit(solution)/shard_map/ppermute | solution.py:109
  201.0 3.0 %collective-permute-start.27 = (bf16[192,1024]{1,0:T(8,128)(2,1)S(1)}, bf16[192,1024]{1,0:T(8,128)(2,1)S(1)}, u32[]{:S(2)}, u32[]{:S(2)}) collective-permute-start(bf16[192,1024]{1,0:T(8,128)(2,1)S(1)} %slice.332), channel_id=1, source_target_pairs={{0,1},{1,0},{2,3},{3,2},{4,5},{5,4},{6,7},{7,6},{8,9},{9,8},{10,11... | collective-permute-start | bytes 1179656 | tf_op jit(solution)/shard_map/ppermute | solution.py:109
  201.1 3.7 %collective-permute-start.24 = (bf16[192,1024]{1,0:T(8,128)(2,1)S(1)}, bf16[192,1024]{1,0:T(8,128)(2,1)S(1)}, u32[]{:S(2)}, u32[]{:S(2)}) collective-permute-start(bf16[192,1024]{1,0:T(8,128)(2,1)S(1)} %slice.333), channel_id=1, source_target_pairs={{0,1},{1,0},{2,3},{3,2},{4,5},{5,4},{6,7},{7,6},{8,9},{9,8},{10,11... | collective-permute-start | bytes 1179656 | tf_op jit(solution)/shard_map/ppermute | solution.py:109
  201.7 7.8 %collective-permute-start.22 = (bf16[192,512]{1,0:T(8,128)(2,1)S(1)}, bf16[192,512]{1,0:T(8,128)(2,1)S(1)}, u32[]{:S(2)}, u32[]{:S(2)}) collective-permute-start(bf16[192,512]{1,0:T(8,128)(2,1)S(1)} %slice.338), channel_id=1, source_target_pairs={{0,2},{1,3},{2,0},{3,1},{4,6},{5,7},{6,4},{7,5},{8,10},{9,11},{10,... | collective-permute-start | bytes 589832 | tf_op jit(solution)/shard_map/ppermute | solution.py:109
  202.5 23.5 %collective-permute-start.31 = (bf16[192,512]{1,0:T(8,128)(2,1)S(1)}, bf16[192,512]{1,0:T(8,128)(2,1)S(1)}, u32[]{:S(2)}, u32[]{:S(2)}) collective-permute-start(bf16[192,512]{1,0:T(8,128)(2,1)S(1)} %slice.335), channel_id=1, source_target_pairs={{0,2},{1,3},{2,0},{3,1},{4,6},{5,7},{6,4},{7,5},{8,10},{9,11},{10,... | collective-permute-start | bytes 589832 | tf_op jit(solution)/shard_map/ppermute | solution.py:109
  204.2 13.8 %collective-permute-start.28 = (bf16[192,512]{1,0:T(8,128)(2,1)S(1)}, bf16[192,512]{1,0:T(8,128)(2,1)S(1)}, u32[]{:S(2)}, u32[]{:S(2)}) collective-permute-start(bf16[192,512]{1,0:T(8,128)(2,1)S(1)} %slice.336), channel_id=1, source_target_pairs={{0,2},{1,3},{2,0},{3,1},{4,6},{5,7},{6,4},{7,5},{8,10},{9,11},{10,... | collective-permute-start | bytes 589832 | tf_op jit(solution)/shard_map/ppermute | solution.py:109
  205.0 16.3 %collective-permute-start.25 = (bf16[192,512]{1,0:T(8,128)(2,1)S(1)}, bf16[192,512]{1,0:T(8,128)(2,1)S(1)}, u32[]{:S(2)}, u32[]{:S(2)}) collective-permute-start(bf16[192,512]{1,0:T(8,128)(2,1)S(1)} %slice.337), channel_id=1, source_target_pairs={{0,2},{1,3},{2,0},{3,1},{4,6},{5,7},{6,4},{7,5},{8,10},{9,11},{10,... | collective-permute-start | bytes 589832 | tf_op jit(solution)/shard_map/ppermute | solution.py:109
  209.6 25.3 %copy-start.1 = (bf16[192,256]{1,0:T(8,128)(2,1)S(1)}, bf16[192,256]{1,0:T(8,128)(2,1)}, u32[]{:S(2)}) copy-start(bf16[192,256]{1,0:T(8,128)(2,1)} %param.15) | copy-start | bytes 294916
  209.6 16.4 %collective-permute-start.23 = (bf16[192,512]{1,0:T(8,128)(2,1)S(1)}, bf16[192,512]{1,0:T(8,128)(2,1)S(1)}, u32[]{:S(2)}, u32[]{:S(2)}) collective-permute-start(bf16[192,512]{1,0:T(8,128)(2,1)S(1)} %fusion.44), channel_id=1, source_target_pairs={{0,12},{4,0},{8,4},{12,8},{1,13},{5,1},{9,5},{13,9},{2,14},{6,2},{... | collective-permute-start | bytes 589832 | tf_op jit(solution)/shard_map/ppermute | solution.py:105
  218.1 8.5 %collective-permute-start.29 = (bf16[192,512]{1,0:T(8,128)(2,1)S(1)}, bf16[192,512]{1,0:T(8,128)(2,1)S(1)}, u32[]{:S(2)}, u32[]{:S(2)}) collective-permute-start(bf16[192,512]{1,0:T(8,128)(2,1)S(1)} %fusion.42), channel_id=1, source_target_pairs={{0,4},{4,8},{8,12},{12,0},{1,5},{5,9},{9,13},{13,1},{2,6},{6,10},{... | collective-permute-start | bytes 589832 | tf_op jit(solution)/shard_map/ppermute | solution.py:105
  221.4 12.6 %collective-permute-start.26 = (bf16[192,512]{1,0:T(8,128)(2,1)S(1)}, bf16[192,512]{1,0:T(8,128)(2,1)S(1)}, u32[]{:S(2)}, u32[]{:S(2)}) collective-permute-start(bf16[192,512]{1,0:T(8,128)(2,1)S(1)} %fusion.43), channel_id=1, source_target_pairs={{0,8},{4,12},{8,0},{12,4},{1,9},{5,13},{9,1},{13,5},{2,10},{6,14},... | collective-permute-start | bytes 589832 | tf_op jit(solution)/shard_map/ppermute | solution.py:105
